TPU v7x, 32 devices: a whole 2x2x4 slice. The times are simulated.
32 devices in a mesh: grp: 2 (over x), sp: 4 (over y, core), tp: 4 (over z).
Axes of the slice: x: 2, y: 2, z: 4, core: 2. Of those that a mesh axis runs over, the one named last changes fastest.
Arguments:
- stream: bfloat16 [2048, 2048], P(('grp', 'sp'), 'tp'), parts along dimension 0, may hold values from -6 to 6
- documents: int32 [2048], P(('grp', 'sp')), parts along dimension 0, may hold values from 0 to 1, never falling along the last dimension, each value on 1 to 768 neighbouring positions
- q_weight: bfloat16 [2, 2048, 2048], P(None, 'sp', 'tp'), may hold values from -0.125 to 0.125
- k_weight: bfloat16 [2, 2048, 2048], P(None, 'sp', 'tp'), may hold values from -0.125 to 0.125
- v_weight: bfloat16 [2, 2048, 2048], P(None, 'sp', 'tp'), may hold values from -0.125 to 0.125
- out_weight: bfloat16 [2, 2048, 2048], P(None, 'sp', 'tp'), may hold values from -0.125 to 0.125
- pre_gain: float32 [2, 2048], replicated, may hold values from 0.1 to 1.9
- post_gain: float32 [2, 2048], P(None, 'tp'), may hold values from 0.1 to 1.9
- offset_bias: float32 [2, 32, 15, 31], P(None, 'tp'), may hold values from -3 to 263
Outputs:
- result_stream: bfloat16 [2048, 2048], P(('grp', 'sp'), 'tp'), parts along dimension 0
There are 2 independent parts, one for each index of `grp`. A program takes and returns all parts, laid end to end along the dimension named above; an argument that names none is the same for every part. Nothing has to cross between parts.
All inputs are finite; a program needn't handle non-finite values.
Results may differ from a plain program's by a relative error of at most 0.02.
Values may be sent and summed in bfloat16 or wider, within the bound.
A program may use at most 128 MiB of HBM per device.

v0:
```python
import functools

import jax
import jax.numpy as jnp
from jax import lax
from jax.experimental import pallas as pl
from jax.experimental.pallas import tpu as pltpu
from jax.sharding import PartitionSpec as P

HEAD_DIM = 64
GRID_W = 64
NA_ROWS = 8
NA_COLS = 16
HALF = NA_ROWS // 2
HALO = HALF * GRID_W
EPS = 1e-06
MESH = pl.DeviceIdType.MESH
F32 = jnp.float32
BF16 = jnp.bfloat16


def kernel(
    n_sp, n_tp, layers, tokens,
    x_ref, docq_ref, dock_ref, wq_ref, wk_ref, wv_ref, wo_ref, pre_ref, post_ref, tab_ref,
    out_ref,
    w_full, x_full, x_scaled, q_buf, k_ext, v_ext, d_ext, att, part, rs_buf, res, sq_own, sq_buf,
    bias, dmask,
    wl_sem, wy_send, wy_recv, wm_send, wm_recv, wf_send, wf_recv,
    xl_sem, x_send, x_recv, d_local, d_send, d_recv, h_send, h_recv, r_send, r_recv, s_send, s_recv,
):
    weights = (wq_ref, wk_ref, wv_ref, wo_ref)
    sp, tp = lax.axis_index("sp"), lax.axis_index("tp")
    n_y = n_sp // 2
    y, core = sp // 2, sp % 2
    mate = y * 2 + (1 - core)
    feats = x_ref.shape[1]
    width = wq_ref.shape[2]
    rows_w = wq_ref.shape[1]
    rows_dev = tokens // GRID_W
    n_pair = width // 128
    d_model = n_tp * feats

    def tp_at(shift):
        return (tp + shift) % n_tp

    def rows_of(owner):
        return pl.ds(pl.multiple_of(owner * rows_w, rows_w), rows_w)

    def remote(src, dst, send, recv, target):
        return pltpu.make_async_remote_copy(
            src_ref=src, dst_ref=dst, send_sem=send, recv_sem=recv,
            device_id=target, device_id_type=MESH,
        )

    barrier = pltpu.get_barrier_semaphore()
    for shift in range(1, n_tp):
        pl.semaphore_signal(barrier, inc=1, device_id={"tp": tp_at(shift)}, device_id_type=MESH)
    for shift in range(1, n_sp):
        pl.semaphore_signal(
            barrier, inc=1, device_id={"sp": (sp + shift) % n_sp}, device_id_type=MESH
        )
    pl.semaphore_wait(barrier, n_tp + n_sp - 2)

    def y_copy(slot, shift):
        mine = w_full.at[slot, rows_of(sp)]
        return remote(
            weights[slot % 4].at[slot // 4], mine, wy_send.at[slot, shift], wy_recv.at[slot, shift],
            {"sp": ((y + shift) % n_y) * 2 + core},
        )

    def mate_copy(slot):
        return remote(
            weights[slot % 4].at[slot // 4], w_full.at[slot, rows_of(sp)],
            wm_send.at[slot], wm_recv.at[slot], {"sp": mate},
        )

    def local_copy(slot):
        return pltpu.make_async_copy(
            weights[slot % 4].at[slot // 4], w_full.at[slot, rows_of(sp)], wl_sem.at[slot]
        )

    def forward_copy(slot, shift):
        block = w_full.at[slot, rows_of(((y - shift + n_y) % n_y) * 2 + core)]
        return remote(
            block, block, wf_send.at[slot, shift], wf_recv.at[slot, shift], {"sp": mate}
        )

    def start_weight(slot):
        for shift in range(1, n_y):
            y_copy(slot, shift).start()
        mate_copy(slot).start()
        local_copy(slot).start()

    def forward_weight(slot):
        for shift in range(1, n_y):
            y_copy(slot, shift).wait_recv()
            forward_copy(slot, shift).start()

    def finish_weight(slot):
        local_copy(slot).wait()
        mate_copy(slot).wait_recv()
        for shift in range(1, n_y):
            forward_copy(slot, shift).wait_recv()

    def drain_weight(slot):
        mate_copy(slot).wait_send()
        for shift in range(1, n_y):
            y_copy(slot, shift).wait_send()
            forward_copy(slot, shift).wait_send()

    def x_copy(layer, shift, source):
        return remote(
            source, x_full.at[layer, tp], x_send.at[layer, shift], x_recv.at[layer, shift],
            {"tp": tp_at(shift)},
        )

    def doc_copy(side):
        if side == 0:
            src, dst, target = dock_ref.at[pl.ds(rows_dev - HALF, HALF)], d_ext.at[pl.ds(0, HALF)], sp + 1
        else:
            src, dst, target = dock_ref.at[pl.ds(0, HALF)], d_ext.at[pl.ds(HALF + rows_dev, HALF)], sp - 1
        return remote(src, dst, d_send.at[side], d_recv.at[side], {"sp": target})

    def halo_copy(layer, side, which):
        buf = (k_ext, v_ext)[which]
        if side == 0:
            src, dst, target = tokens, 0, sp + 1
        else:
            src, dst, target = HALO, HALO + tokens, sp - 1
        return remote(
            buf.at[layer, pl.ds(src, HALO)], buf.at[layer, pl.ds(dst, HALO)],
            h_send.at[layer, side, which], h_recv.at[layer, side, which], {"sp": target},
        )

    has_next, has_prev = sp < n_sp - 1, sp > 0

    for slot in range(3):
        start_weight(slot)
    x_local = pltpu.make_async_copy(x_ref, x_full.at[0, tp], xl_sem)
    x_local.start()
    for shift in range(1, n_tp):
        x_copy(0, shift, x_ref).start()
    d_own = pltpu.make_async_copy(dock_ref, d_ext.at[pl.ds(HALF, rows_dev)], d_local)
    d_own.start()

    @pl.when(has_next)
    def _():
        doc_copy(0).start()

    @pl.when(has_prev)
    def _():
        doc_copy(1).start()

    q_ids = lax.broadcasted_iota(jnp.int32, (GRID_W, 128), 0)
    lanes = lax.broadcasted_iota(jnp.int32, (GRID_W, 128), 1)
    key_col = lanes % GRID_W
    first_col = jnp.clip(q_ids - NA_COLS // 2, 0, GRID_W - NA_COLS)
    col_ok = (key_col >= first_col) & (key_col < first_col + NA_COLS)
    low_half = lanes < GRID_W
    n_off = 2 * NA_ROWS - 2

    def expand(step, _):
        group, offset = step // n_off, step % n_off
        pair_rows = tab_ref[group, offset]
        for half in range(2):
            row = jnp.broadcast_to(pair_rows[half:half + 1], (GRID_W, 128))
            skew = pltpu.roll(row, 128 - (NA_COLS - 1), 1, stride=1, stride_axis=0)
            bias[group, offset, half * GRID_W:(half + 1) * GRID_W] = jnp.where(
                col_ok, skew, -jnp.inf
            )
        return 0

    lax.fori_loop(0, layers * n_pair * n_off, expand, 0)

    d_own.wait()

    @pl.when(has_next)
    def _():
        doc_copy(0).wait_send()
        doc_copy(1).wait_recv()

    @pl.when(has_prev)
    def _():
        doc_copy(1).wait_send()
        doc_copy(0).wait_recv()

    first_row = sp * rows_dev

    def window(row):
        start = jnp.clip(first_row + row - HALF, 0, rows_dev * n_sp - NA_ROWS)
        return start - first_row + HALF

    for row in range(rows_dev):
        q_doc = docq_ref[row * GRID_W:(row + 1) * GRID_W, :]
        for pair in range(NA_ROWS // 2):
            at = window(row) + 2 * pair
            k_doc = jnp.where(
                low_half,
                jnp.broadcast_to(d_ext[at][0:1], (GRID_W, 128)),
                jnp.broadcast_to(d_ext[at + 1][0:1], (GRID_W, 128)),
            )
            value = jnp.where(k_doc == q_doc, 0.0, -jnp.inf).astype(F32)
            dmask[row, pair, 0:GRID_W] = value
            dmask[row, pair, GRID_W:2 * GRID_W] = value

    x_local.wait()

    for layer in range(layers):
        base = 4 * layer
        for shift in range(1, n_tp):
            x_copy(layer, shift, x_ref).wait_recv()
        total = jnp.zeros((tokens, 1), F32)
        for block in range(n_tp):
            wide = x_full[layer, block].astype(F32)
            total = total + jnp.sum(wide * wide, axis=1, keepdims=True)
            gain = pre_ref[layer:layer + 1, block * feats:(block + 1) * feats]
            x_scaled[:, block * feats:(block + 1) * feats] = (wide * gain).astype(BF16)
        inverse = lax.rsqrt(total / d_model + EPS)

        for slot in range(base, base + 3):
            forward_weight(slot)
        for which in (1, 2, 0):
            finish_weight(base + which)
            product = jnp.dot(x_scaled[...], w_full[base + which], preferred_element_type=F32)
            rounded = (product * inverse).astype(BF16)
            if which == 0:
                q_buf[...] = rounded * jnp.asarray(HEAD_DIM ** -0.5, BF16)
            else:
                buf = (k_ext, v_ext)[which - 1]
                buf[layer, HALO:HALO + tokens] = rounded

                @pl.when(has_next)
                def _():
                    halo_copy(layer, 0, which - 1).start()

                @pl.when(has_prev)
                def _():
                    halo_copy(layer, 1, which - 1).start()

        start_weight(base + 3)
        if layer + 1 < layers:
            for slot in range(base + 4, base + 7):
                start_weight(slot)

        for which in range(2):
            @pl.when(has_next)
            def _():
                halo_copy(layer, 1, which).wait_recv()

            @pl.when(has_prev)
            def _():
                halo_copy(layer, 0, which).wait_recv()

        def attend(step, _):
            pair, row = step // rows_dev, step % rows_dev
            begin = window(row)
            cols = pl.ds(pl.multiple_of(pair * 128, 128), 128)
            q_rows = pl.ds(pl.multiple_of(row * GRID_W, GRID_W), GRID_W)
            keys = pl.ds(pl.multiple_of(begin * GRID_W, GRID_W), NA_ROWS * GRID_W)
            q2 = q_buf[q_rows, cols]
            zero = jnp.zeros_like(q2)
            stacked = jnp.concatenate(
                [jnp.where(low_half, q2, zero), jnp.where(low_half, zero, q2)], axis=0
            )
            k2 = k_ext[layer, keys, cols]
            scores = lax.dot_general(
                stacked, k2, (((1,), (1,)), ((), ())), preferred_element_type=F32
            )
            offset = begin - row + NA_ROWS - 1 - HALF
            pieces = []
            for at in range(NA_ROWS // 2):
                pieces.append(
                    scores[:, at * 128:(at + 1) * 128]
                    + bias[layer * n_pair + pair, offset + 2 * at]
                    + dmask[row, at]
                )
            full = jnp.concatenate(pieces, axis=1)
            top = jnp.max(full, axis=1, keepdims=True)
            grown = jnp.exp(full - top)
            share = 1.0 / jnp.sum(grown, axis=1, keepdims=True)
            probs = (grown * share).astype(BF16)
            mixed = jnp.dot(probs, v_ext[layer, keys, cols], preferred_element_type=F32)
            att[q_rows, cols] = jnp.where(low_half, mixed[:GRID_W], mixed[GRID_W:]).astype(BF16)
            return 0

        lax.fori_loop(0, n_pair * rows_dev, attend, 0)

        forward_weight(base + 3)
        finish_weight(base + 3)

        def r_copy(shift):
            return remote(
                part.at[layer, tp_at(shift)], rs_buf.at[layer, tp],
                r_send.at[layer, shift], r_recv.at[layer, shift], {"tp": tp_at(shift)},
            )

        for shift in list(range(1, n_tp)) + [0]:
            block = tp_at(shift)
            w_rows = pl.ds(pl.multiple_of(block * feats, feats), feats)
            product = lax.dot_general(
                att[...], w_full[base + 3, w_rows], (((1,), (1,)), ((), ())),
                preferred_element_type=F32,
            )
            part[layer, block] = product.astype(BF16)
            if shift:
                r_copy(shift).start()
        branch = part[layer, tp].astype(F32)
        for shift in range(1, n_tp):
            r_copy(shift).wait_recv()
            branch = branch + rs_buf[layer, tp_at(n_tp - shift)].astype(F32)
        squares = jnp.sum(branch * branch, axis=1, keepdims=True)
        flat = jnp.transpose(jnp.broadcast_to(squares, (tokens, 128)))
        sq_own[layer] = flat[0:8]

        def s_copy(shift):
            return remote(
                sq_own.at[layer], sq_buf.at[layer, tp],
                s_send.at[layer, shift], s_recv.at[layer, shift], {"tp": tp_at(shift)},
            )

        for shift in range(1, n_tp):
            s_copy(shift).start()
        summed = sq_own[layer]
        for shift in range(1, n_tp):
            s_copy(shift).wait_recv()
            summed = summed + sq_buf[layer, tp_at(n_tp - shift)]
        column = jnp.transpose(jnp.broadcast_to(summed[0:1], (128, tokens)))[:, 0:1]
        out_inverse = lax.rsqrt(column / d_model + EPS)
        before = x_ref[...] if layer == 0 else res[layer - 1]
        after = (
            before.astype(F32) + branch * out_inverse * post_ref[layer:layer + 1, :]
        ).astype(BF16)
        if layer + 1 < layers:
            res[layer] = after
            x_full[layer + 1, tp] = after
            for shift in range(1, n_tp):
                x_copy(layer + 1, shift, res.at[layer]).start()
        else:
            out_ref[...] = after
        for shift in range(1, n_tp):
            x_copy(layer, shift, x_ref).wait_send()
            r_copy(shift).wait_send()
            s_copy(shift).wait_send()
        for which in range(2):
            @pl.when(has_next)
            def _():
                halo_copy(layer, 0, which).wait_send()

            @pl.when(has_prev)
            def _():
                halo_copy(layer, 1, which).wait_send()
        for slot in range(base, base + 4):
            drain_weight(slot)


def shards(
    stream, documents, q_weight, k_weight, v_weight, out_weight, pre_gain, post_gain, offset_bias
):
    n_sp, n_tp = lax.axis_size("sp"), lax.axis_size("tp")
    tokens, feats = stream.shape
    layers, rows_w, width = q_weight.shape
    rows_dev = tokens // GRID_W
    n_pair = width // 128
    d_model = feats * n_tp
    n_off = 2 * NA_ROWS - 2
    doc_query = jnp.broadcast_to(documents[:, None], (tokens, 128))
    grid_docs = documents.reshape(rows_dev, 1, GRID_W)
    doc_key = jnp.broadcast_to(
        jnp.concatenate([grid_docs, grid_docs], axis=2), (rows_dev, 8, 2 * GRID_W)
    )
    table = jnp.pad(offset_bias, ((0, 0), (0, 0), (0, 0), (0, GRID_W - 2 * NA_COLS + 1)))
    table = jnp.concatenate([table[:, :, :-1], table[:, :, 1:]], axis=3)
    table = table.reshape(layers * n_pair, 2, n_off, 128).transpose(0, 2, 1, 3)
    n_y = n_sp // 2
    slots = 4 * layers
    ext = tokens + 2 * HALO
    dma = pltpu.SemaphoreType.DMA
    vmem = pl.BlockSpec(memory_space=pltpu.VMEM)
    hbm = pl.BlockSpec(memory_space=pl.ANY)
    return pl.pallas_call(
        functools.partial(kernel, n_sp, n_tp, layers, tokens),
        out_shape=jax.ShapeDtypeStruct((tokens, feats), BF16),
        in_specs=[vmem] * 3 + [hbm] * 4 + [vmem] * 3,
        out_specs=vmem,
        scratch_shapes=[
            pltpu.VMEM((slots, d_model, width), BF16),
            pltpu.VMEM((layers, n_tp, tokens, feats), BF16),
            pltpu.VMEM((tokens, d_model), BF16),
            pltpu.VMEM((tokens, width), BF16),
            pltpu.VMEM((layers, ext, width), BF16),
            pltpu.VMEM((layers, ext, width), BF16),
            pltpu.VMEM((rows_dev + 2 * HALF, 8, 128), jnp.int32),
            pltpu.VMEM((tokens, width), BF16),
            pltpu.VMEM((layers, n_tp, tokens, feats), BF16),
            pltpu.VMEM((layers, n_tp, tokens, feats), BF16),
            pltpu.VMEM((layers, tokens, feats), BF16),
            pltpu.VMEM((layers, 8, tokens), F32),
            pltpu.VMEM((layers, n_tp, 8, tokens), F32),
            pltpu.VMEM((layers * n_pair, n_off, 128, 128), F32),
            pltpu.VMEM((rows_dev, NA_ROWS // 2, 128, 128), F32),
            dma((slots,)),
            dma((slots, n_y)), dma((slots, n_y)),
            dma((slots,)), dma((slots,)),
            dma((slots, n_y)), dma((slots, n_y)),
            dma,
            dma((layers, n_tp)), dma((layers, n_tp)),
            dma, dma((2,)), dma((2,)),
            dma((layers, 2, 2)), dma((layers, 2, 2)),
            dma((layers, n_tp)), dma((layers, n_tp)),
            dma((layers, n_tp)), dma((layers, n_tp)),
        ],
        compiler_params=pltpu.CompilerParams(
            collective_id=0, has_side_effects=True, vmem_limit_bytes=60 * 1024 * 1024
        ),
    )(
        stream, doc_query, doc_key, q_weight, k_weight, v_weight, out_weight,
        pre_gain, post_gain, table,
    )


def solution(mesh):
    in_specs = (
        P(("grp", "sp"), "tp"),
        P(("grp", "sp")),
        P(None, "sp", "tp"),
        P(None, "sp", "tp"),
        P(None, "sp", "tp"),
        P(None, "sp", "tp"),
        P(),
        P(None, "tp"),
        P(None, "tp", None, None),
    )
    out_specs = P(("grp", "sp"), "tp")
    return jax.shard_map(shards, mesh=mesh, in_specs=in_specs, out_specs=out_specs, check_vma=False)
```

profile of v0, /device:TPU:4, one launch (start us, length us, event | category | flops | bytes accessed | tf_op | source)
XLA Modules:
  0.0 176.5 jit_solution(7820919210331229881)
XLA Ops:
  0.0 0.0 copy-start
  0.0 0.8 reshape.7
  0.8 0.1 add_bitcast_fusion
  0.9 0.6 broadcast_in_dim.15.dock_ref
  1.5 1.4 broadcast_in_dim.6.docq_ref
  2.9 0.0 copy-done
  2.9 0.1 pad_maximum_fusion
  3.0 0.7 copy.15
  3.7 171.1 %shard_map.91 = bf16[256,512]{1,0:T(8,128)(2,1)} custom-call(bf16[256,512]{1,0:T(8,128)(2,1)} %x_ref.1, s32[256,128]{1,0:T(8,128)} %broadcast_in_dim.6.docq_ref, s32[4,8,128]{2,1,0:T(8,128)} %broadcast_in_dim.15.dock_ref, bf16[2,512,512]{2,1,0:T(8,128)(2,1)} %wq_ref.1, bf16[2,512,512]{2,1,0:T(8,128)(2,1)} %wk_ref.1, bf16[2,512,512]{2,1,0:T(8,128)(2,1)} %wv_ref.1, ...), custom_call_target="tpu_custom_call" | custom-call | tf_op jit(solution)/shard_map/pallas_call | solution.py:380
  174.8 1.7 copy.17
  (1 shorter events, 0.0 us)
Async XLA Ops:
  0.0 2.9 %copy-start = (f32[2,8,15,31]{3,1,2,0:T(8,128)S(1)}, f32[2,8,15,31]{3,1,2,0:T(8,128)}, u32[]{:S(2)}) copy-start(f32[2,8,15,31]{3,1,2,0:T(8,128)} %param.17) | copy-start | bytes 89284
where the time goes:
time: 177 us; the launch traced here: 176 us
  Pallas kernels  171 us (97%)
  local copies, waits for them, and re-layouts  5.21 us (3%)
    pallas_call x1, Pallas kernels, shards(): pl.pallas_call(functools.partial(kernel, n_sp, n_tp, layers, tokens), out...  171 us

commit v1 on v0

--- a/solution.py
+++ b/solution.py
@@ -20,16 +20,16 @@
 
 
 def kernel(
-    n_sp, n_tp, layers, tokens,
+    n_sp, n_tp, n_grp, layers, tokens,
     x_ref, docq_ref, dock_ref, wq_ref, wk_ref, wv_ref, wo_ref, pre_ref, post_ref, tab_ref,
     out_ref,
-    w_full, x_full, x_scaled, q_buf, k_ext, v_ext, d_ext, att, part, rs_buf, res, sq_own, sq_buf,
+    w_full, x_full, x_scaled, q_buf, k_ext, v_ext, d_ext, part, rs_buf, res, sq_own, sq_buf,
     bias, dmask,
-    wl_sem, wy_send, wy_recv, wm_send, wm_recv, wf_send, wf_recv,
+    wl_sem, wy_send, wy_recv, wm_send, wm_recv, wf_send, wf_recv, wx_send, wx_recv,
     xl_sem, x_send, x_recv, d_local, d_send, d_recv, h_send, h_recv, r_send, r_recv, s_send, s_recv,
 ):
     weights = (wq_ref, wk_ref, wv_ref, wo_ref)
-    sp, tp = lax.axis_index("sp"), lax.axis_index("tp")
+    sp, tp, grp = lax.axis_index("sp"), lax.axis_index("tp"), lax.axis_index("grp")
     n_y = n_sp // 2
     y, core = sp // 2, sp % 2
     mate = y * 2 + (1 - core)
@@ -43,8 +43,13 @@
     def tp_at(shift):
         return (tp + shift) % n_tp
 
+    piece = rows_w // n_grp
+
     def rows_of(owner):
         return pl.ds(pl.multiple_of(owner * rows_w, rows_w), rows_w)
+
+    def piece_of(owner, index):
+        return pl.ds(pl.multiple_of(owner * rows_w + index * piece, piece), piece)
 
     def remote(src, dst, send, recv, target):
         return pltpu.make_async_remote_copy(
@@ -59,12 +64,17 @@
         pl.semaphore_signal(
             barrier, inc=1, device_id={"sp": (sp + shift) % n_sp}, device_id_type=MESH
         )
-    pl.semaphore_wait(barrier, n_tp + n_sp - 2)
+    for shift in range(1, n_grp):
+        pl.semaphore_signal(
+            barrier, inc=1, device_id={"grp": (grp + shift) % n_grp}, device_id_type=MESH
+        )
+    pl.semaphore_wait(barrier, n_tp + n_sp + n_grp - 3)
 
     def y_copy(slot, shift):
-        mine = w_full.at[slot, rows_of(sp)]
-        return remote(
-            weights[slot % 4].at[slot // 4], mine, wy_send.at[slot, shift], wy_recv.at[slot, shift],
+        own = pl.ds(pl.multiple_of(grp * piece, piece), piece)
+        return remote(
+            weights[slot % 4].at[slot // 4, own], w_full.at[slot, piece_of(sp, grp)],
+            wy_send.at[slot, shift], wy_recv.at[slot, shift],
             {"sp": ((y + shift) % n_y) * 2 + core},
         )
 
@@ -79,10 +89,22 @@
             weights[slot % 4].at[slot // 4], w_full.at[slot, rows_of(sp)], wl_sem.at[slot]
         )
 
-    def forward_copy(slot, shift):
-        block = w_full.at[slot, rows_of(((y - shift + n_y) % n_y) * 2 + core)]
-        return remote(
-            block, block, wf_send.at[slot, shift], wf_recv.at[slot, shift], {"sp": mate}
+    def arrived(slot, shift, turn):
+        owner = ((y - shift + n_y) % n_y) * 2 + core
+        return w_full.at[slot, piece_of(owner, (grp - turn + n_grp) % n_grp)]
+
+    def forward_copy(slot, shift, turn):
+        block = arrived(slot, shift, turn)
+        return remote(
+            block, block, wf_send.at[slot, shift, turn], wf_recv.at[slot, shift, turn],
+            {"sp": mate},
+        )
+
+    def x_link_copy(slot, shift, turn):
+        block = arrived(slot, shift, 0)
+        return remote(
+            block, block, wx_send.at[slot, shift, turn], wx_recv.at[slot, shift, turn],
+            {"grp": (grp + turn) % n_grp},
         )
 
     def start_weight(slot):
@@ -91,22 +113,34 @@
         mate_copy(slot).start()
         local_copy(slot).start()
 
-    def forward_weight(slot):
+    def pass_on(slot):
         for shift in range(1, n_y):
             y_copy(slot, shift).wait_recv()
-            forward_copy(slot, shift).start()
+            for turn in range(1, n_grp):
+                x_link_copy(slot, shift, turn).start()
+            forward_copy(slot, shift, 0).start()
+
+    def pass_across(slot):
+        for shift in range(1, n_y):
+            for turn in range(1, n_grp):
+                x_link_copy(slot, shift, turn).wait_recv()
+                forward_copy(slot, shift, turn).start()
 
     def finish_weight(slot):
         local_copy(slot).wait()
         mate_copy(slot).wait_recv()
         for shift in range(1, n_y):
-            forward_copy(slot, shift).wait_recv()
+            for turn in range(n_grp):
+                forward_copy(slot, shift, turn).wait_recv()
 
     def drain_weight(slot):
         mate_copy(slot).wait_send()
         for shift in range(1, n_y):
             y_copy(slot, shift).wait_send()
-            forward_copy(slot, shift).wait_send()
+            for turn in range(n_grp):
+                forward_copy(slot, shift, turn).wait_send()
+            for turn in range(1, n_grp):
+                x_link_copy(slot, shift, turn).wait_send()
 
     def x_copy(layer, shift, source):
         return remote(
@@ -134,7 +168,8 @@
 
     has_next, has_prev = sp < n_sp - 1, sp > 0
 
-    for slot in range(3):
+    order = (1, 2, 0, 3)
+    for slot in order:
         start_weight(slot)
     x_local = pltpu.make_async_copy(x_ref, x_full.at[0, tp], xl_sem)
     x_local.start()
@@ -203,6 +238,10 @@
             dmask[row, pair, 0:GRID_W] = value
             dmask[row, pair, GRID_W:2 * GRID_W] = value
 
+    for slot in order[:3]:
+        pass_on(slot)
+    for slot in order[:2]:
+        pass_across(slot)
     x_local.wait()
 
     for layer in range(layers):
@@ -217,9 +256,9 @@
             x_scaled[:, block * feats:(block + 1) * feats] = (wide * gain).astype(BF16)
         inverse = lax.rsqrt(total / d_model + EPS)
 
-        for slot in range(base, base + 3):
-            forward_weight(slot)
-        for which in (1, 2, 0):
+        if layer == 0:
+            pass_across(order[2])
+        for which in order[:3]:
             finish_weight(base + which)
             product = jnp.dot(x_scaled[...], w_full[base + which], preferred_element_type=F32)
             rounded = (product * inverse).astype(BF16)
@@ -237,10 +276,12 @@
                 def _():
                     halo_copy(layer, 1, which - 1).start()
 
-        start_weight(base + 3)
         if layer + 1 < layers:
-            for slot in range(base + 4, base + 7):
-                start_weight(slot)
+            for slot in order:
+                start_weight(base + 4 + slot)
+        if layer == 0:
+            pass_on(3)
+            pass_across(3)
 
         for which in range(2):
             @pl.when(has_next)
@@ -251,62 +292,71 @@
             def _():
                 halo_copy(layer, 0, which).wait_recv()
 
-        def attend(step, _):
-            pair, row = step // rows_dev, step % rows_dev
+        finish_weight(base + 3)
+
+        def r_copy(row, shift):
+            here = pl.ds(pl.multiple_of(row * GRID_W, GRID_W), GRID_W)
+            return remote(
+                part.at[layer, tp_at(shift), here], rs_buf.at[layer, tp, here],
+                r_send.at[layer, row, shift], r_recv.at[layer, row, shift],
+                {"tp": tp_at(shift)},
+            )
+
+        def attend(row, _):
             begin = window(row)
-            cols = pl.ds(pl.multiple_of(pair * 128, 128), 128)
             q_rows = pl.ds(pl.multiple_of(row * GRID_W, GRID_W), GRID_W)
             keys = pl.ds(pl.multiple_of(begin * GRID_W, GRID_W), NA_ROWS * GRID_W)
-            q2 = q_buf[q_rows, cols]
-            zero = jnp.zeros_like(q2)
-            stacked = jnp.concatenate(
-                [jnp.where(low_half, q2, zero), jnp.where(low_half, zero, q2)], axis=0
-            )
-            k2 = k_ext[layer, keys, cols]
-            scores = lax.dot_general(
-                stacked, k2, (((1,), (1,)), ((), ())), preferred_element_type=F32
-            )
             offset = begin - row + NA_ROWS - 1 - HALF
-            pieces = []
-            for at in range(NA_ROWS // 2):
-                pieces.append(
-                    scores[:, at * 128:(at + 1) * 128]
-                    + bias[layer * n_pair + pair, offset + 2 * at]
-                    + dmask[row, at]
+            attended = []
+            for pair in range(n_pair):
+                cols = slice(pair * 128, (pair + 1) * 128)
+                q2 = q_buf[q_rows, cols]
+                zero = jnp.zeros_like(q2)
+                stacked = jnp.concatenate(
+                    [jnp.where(low_half, q2, zero), jnp.where(low_half, zero, q2)], axis=0
                 )
-            full = jnp.concatenate(pieces, axis=1)
-            top = jnp.max(full, axis=1, keepdims=True)
-            grown = jnp.exp(full - top)
-            share = 1.0 / jnp.sum(grown, axis=1, keepdims=True)
-            probs = (grown * share).astype(BF16)
-            mixed = jnp.dot(probs, v_ext[layer, keys, cols], preferred_element_type=F32)
-            att[q_rows, cols] = jnp.where(low_half, mixed[:GRID_W], mixed[GRID_W:]).astype(BF16)
+                k2 = k_ext[layer, keys, cols]
+                scores = lax.dot_general(
+                    stacked, k2, (((1,), (1,)), ((), ())), preferred_element_type=F32
+                )
+                pieces = []
+                for at in range(NA_ROWS // 2):
+                    pieces.append(
+                        scores[:, at * 128:(at + 1) * 128]
+                        + bias[layer * n_pair + pair, offset + 2 * at]
+                        + dmask[row, at]
+                    )
+                full = jnp.concatenate(pieces, axis=1)
+                top = jnp.max(full, axis=1, keepdims=True)
+                grown = jnp.exp(full - top)
+                share = 1.0 / jnp.sum(grown, axis=1, keepdims=True)
+                probs = (grown * share).astype(BF16)
+                mixed = jnp.dot(probs, v_ext[layer, keys, cols], preferred_element_type=F32)
+                attended.append(
+                    jnp.where(low_half, mixed[:GRID_W], mixed[GRID_W:]).astype(BF16)
+                )
+            attended = jnp.concatenate(attended, axis=1)
+            for shift in list(range(1, n_tp)) + [0]:
+                block = tp_at(shift)
+                w_rows = pl.ds(pl.multiple_of(block * feats, feats), feats)
+                product = lax.dot_general(
+                    attended, w_full[base + 3, w_rows], (((1,), (1,)), ((), ())),
+                    preferred_element_type=F32,
+                )
+                part[layer, block, q_rows] = product.astype(BF16)
+                if shift:
+                    r_copy(row, shift).start()
             return 0
 
-        lax.fori_loop(0, n_pair * rows_dev, attend, 0)
-
-        forward_weight(base + 3)
-        finish_weight(base + 3)
-
-        def r_copy(shift):
-            return remote(
-                part.at[layer, tp_at(shift)], rs_buf.at[layer, tp],
-                r_send.at[layer, shift], r_recv.at[layer, shift], {"tp": tp_at(shift)},
-            )
-
-        for shift in list(range(1, n_tp)) + [0]:
-            block = tp_at(shift)
-            w_rows = pl.ds(pl.multiple_of(block * feats, feats), feats)
-            product = lax.dot_general(
-                att[...], w_full[base + 3, w_rows], (((1,), (1,)), ((), ())),
-                preferred_element_type=F32,
-            )
-            part[layer, block] = product.astype(BF16)
-            if shift:
-                r_copy(shift).start()
+        lax.fori_loop(0, rows_dev, attend, 0)
+
+        if layer + 1 < layers:
+            for slot in order:
+                pass_on(base + 4 + slot)
         branch = part[layer, tp].astype(F32)
         for shift in range(1, n_tp):
-            r_copy(shift).wait_recv()
+            for row in range(rows_dev):
+                r_copy(row, shift).wait_recv()
             branch = branch + rs_buf[layer, tp_at(n_tp - shift)].astype(F32)
         squares = jnp.sum(branch * branch, axis=1, keepdims=True)
         flat = jnp.transpose(jnp.broadcast_to(squares, (tokens, 128)))
@@ -335,11 +385,14 @@
             x_full[layer + 1, tp] = after
             for shift in range(1, n_tp):
                 x_copy(layer + 1, shift, res.at[layer]).start()
+            for slot in order:
+                pass_across(base + 4 + slot)
         else:
             out_ref[...] = after
         for shift in range(1, n_tp):
             x_copy(layer, shift, x_ref).wait_send()
-            r_copy(shift).wait_send()
+            for row in range(rows_dev):
+                r_copy(row, shift).wait_send()
             s_copy(shift).wait_send()
         for which in range(2):
             @pl.when(has_next)
@@ -356,7 +409,7 @@
 def shards(
     stream, documents, q_weight, k_weight, v_weight, out_weight, pre_gain, post_gain, offset_bias
 ):
-    n_sp, n_tp = lax.axis_size("sp"), lax.axis_size("tp")
+    n_sp, n_tp, n_grp = lax.axis_size("sp"), lax.axis_size("tp"), lax.axis_size("grp")
     tokens, feats = stream.shape
     layers, rows_w, width = q_weight.shape
     rows_dev = tokens // GRID_W
@@ -378,7 +431,7 @@
     vmem = pl.BlockSpec(memory_space=pltpu.VMEM)
     hbm = pl.BlockSpec(memory_space=pl.ANY)
     return pl.pallas_call(
-        functools.partial(kernel, n_sp, n_tp, layers, tokens),
+        functools.partial(kernel, n_sp, n_tp, n_grp, layers, tokens),
         out_shape=jax.ShapeDtypeStruct((tokens, feats), BF16),
         in_specs=[vmem] * 3 + [hbm] * 4 + [vmem] * 3,
         out_specs=vmem,
@@ -390,7 +443,6 @@
             pltpu.VMEM((layers, ext, width), BF16),
             pltpu.VMEM((layers, ext, width), BF16),
             pltpu.VMEM((rows_dev + 2 * HALF, 8, 128), jnp.int32),
-            pltpu.VMEM((tokens, width), BF16),
             pltpu.VMEM((layers, n_tp, tokens, feats), BF16),
             pltpu.VMEM((layers, n_tp, tokens, feats), BF16),
             pltpu.VMEM((layers, tokens, feats), BF16),
@@ -401,12 +453,13 @@
             dma((slots,)),
             dma((slots, n_y)), dma((slots, n_y)),
             dma((slots,)), dma((slots,)),
-            dma((slots, n_y)), dma((slots, n_y)),
+            dma((slots, n_y, n_grp)), dma((slots, n_y, n_grp)),
+            dma((slots, n_y, n_grp)), dma((slots, n_y, n_grp)),
             dma,
             dma((layers, n_tp)), dma((layers, n_tp)),
             dma, dma((2,)), dma((2,)),
             dma((layers, 2, 2)), dma((layers, 2, 2)),
-            dma((layers, n_tp)), dma((layers, n_tp)),
+            dma((layers, rows_dev, n_tp)), dma((layers, rows_dev, n_tp)),
             dma((layers, n_tp)), dma((layers, n_tp)),
         ],
         compiler_params=pltpu.CompilerParams(

time: 177 us -> 145 us (0.82)
  Pallas kernels: 171 us -> 138 us
    pallas_call x1, Pallas kernels: 171 us -> 138 us  [shards(): pl.pallas_call(functools.partial(kernel, n_sp, n_tp, n_grp, layers, token...]
where the time goes in v1:
time: 145 us; the launch traced here: 143 us
  Pallas kernels  138 us (95%)
  local copies, waits for them, and re-layouts  5.21 us (4%)
    pallas_call x1, Pallas kernels, shards(): pl.pallas_call(functools.partial(kernel, n_sp, n_tp, n_grp, layers, token...  138 us

profile of v1, /device:TPU:4, one launch (start us, length us, event | category | flops | bytes accessed | tf_op | source)
XLA Modules:
  0.0 143.2 jit_solution(3353552185999360325)
XLA Ops:
  0.0 0.0 copy-start
  0.0 0.8 reshape.7
  0.8 0.1 add_bitcast_fusion
  0.9 0.6 broadcast_in_dim.15.dock_ref
  1.5 1.4 %broadcast_in_dim.6.docq_ref = s32[256,128]{1,0:T(8,128)} broadcast(s32[256]{0:T(256)} %param.10), dimensions={0} | broadcast | bytes 132096 | tf_op jit(solution)/shard_map/broadcast_in_dim | solution.py:419
  2.9 0.0 copy-done
  2.9 0.1 pad_maximum_fusion
  3.0 0.7 copy.15
  3.7 137.8 %shard_map.91 = bf16[256,512]{1,0:T(8,128)(2,1)} custom-call(bf16[256,512]{1,0:T(8,128)(2,1)} %x_ref.1, s32[256,128]{1,0:T(8,128)} %broadcast_in_dim.6.docq_ref, s32[4,8,128]{2,1,0:T(8,128)} %broadcast_in_dim.15.dock_ref, bf16[2,512,512]{2,1,0:T(8,128)(2,1)} %wq_ref.1, bf16[2,512,512]{2,1,0:T(8,128)(2,1)} %wk_ref.1, bf16[2,512,512]{2,1,0:T(8,128)(2,1)} %wv_ref.1, ...), custom_call_target="tpu_custom_call" | custom-call | tf_op jit(solution)/shard_map/pallas_call | solution.py:433
  141.6 1.7 %copy.17 = bf16[256,512]{1,0:T(8,128)(2,1)} copy(bf16[256,512]{1,0:T(8,128)(2,1)} %shard_map.91) | data formatting | bytes 524288
  (1 shorter events, 0.0 us)
Async XLA Ops:
  0.0 2.9 %copy-start = (f32[2,8,15,31]{3,1,2,0:T(8,128)S(1)}, f32[2,8,15,31]{3,1,2,0:T(8,128)}, u32[]{:S(2)}) copy-start(f32[2,8,15,31]{3,1,2,0:T(8,128)} %param.17) | copy-start | bytes 89284

commit v2 on v1

--- a/solution.py
+++ b/solution.py
@@ -21,7 +21,7 @@
 
 def kernel(
     n_sp, n_tp, n_grp, layers, tokens,
-    x_ref, docq_ref, dock_ref, wq_ref, wk_ref, wv_ref, wo_ref, pre_ref, post_ref, tab_ref,
+    x_ref, dock_ref, wq_ref, wk_ref, wv_ref, wo_ref, pre_ref, post_ref, tab_ref,
     out_ref,
     w_full, x_full, x_scaled, q_buf, k_ext, v_ext, d_ext, part, rs_buf, res, sq_own, sq_buf,
     bias, dmask,
@@ -196,16 +196,21 @@
 
     def expand(step, _):
         group, offset = step // n_off, step % n_off
-        pair_rows = tab_ref[group, offset]
         for half in range(2):
-            row = jnp.broadcast_to(pair_rows[half:half + 1], (GRID_W, 128))
+            first = tab_ref[group * 2 + half, pl.ds(offset, 1)]
+            second = tab_ref[group * 2 + half, pl.ds(offset + 1, 1)]
+            row = jnp.broadcast_to(first + pltpu.roll(second, GRID_W, 1), (GRID_W, 128))
             skew = pltpu.roll(row, 128 - (NA_COLS - 1), 1, stride=1, stride_axis=0)
             bias[group, offset, half * GRID_W:(half + 1) * GRID_W] = jnp.where(
                 col_ok, skew, -jnp.inf
             )
         return 0
 
-    lax.fori_loop(0, layers * n_pair * n_off, expand, 0)
+    def expand_layer(layer):
+        lax.fori_loop(layer * n_pair * n_off, (layer + 1) * n_pair * n_off, expand, 0)
+
+    expand_layer(0)
+    pass_on(order[0])
 
     d_own.wait()
 
@@ -226,7 +231,8 @@
         return start - first_row + HALF
 
     for row in range(rows_dev):
-        q_doc = docq_ref[row * GRID_W:(row + 1) * GRID_W, :]
+        own_docs = jnp.broadcast_to(dock_ref[row][0:1].astype(F32), (128, 128))
+        q_doc = jnp.transpose(own_docs)[0:GRID_W]
         for pair in range(NA_ROWS // 2):
             at = window(row) + 2 * pair
             k_doc = jnp.where(
@@ -234,29 +240,32 @@
                 jnp.broadcast_to(d_ext[at][0:1], (GRID_W, 128)),
                 jnp.broadcast_to(d_ext[at + 1][0:1], (GRID_W, 128)),
             )
-            value = jnp.where(k_doc == q_doc, 0.0, -jnp.inf).astype(F32)
+            value = jnp.where(k_doc.astype(F32) == q_doc, 0.0, -jnp.inf).astype(F32)
             dmask[row, pair, 0:GRID_W] = value
             dmask[row, pair, GRID_W:2 * GRID_W] = value
 
-    for slot in order[:3]:
-        pass_on(slot)
-    for slot in order[:2]:
-        pass_across(slot)
+    pass_on(order[1])
+    pass_across(order[0])
     x_local.wait()
 
     for layer in range(layers):
         base = 4 * layer
-        for shift in range(1, n_tp):
-            x_copy(layer, shift, x_ref).wait_recv()
         total = jnp.zeros((tokens, 1), F32)
-        for block in range(n_tp):
+        for shift in range(n_tp):
+            if shift:
+                x_copy(layer, shift, x_ref).wait_recv()
+            block = tp_at(n_tp - shift)
+            span = pl.ds(pl.multiple_of(block * feats, feats), feats)
             wide = x_full[layer, block].astype(F32)
             total = total + jnp.sum(wide * wide, axis=1, keepdims=True)
-            gain = pre_ref[layer:layer + 1, block * feats:(block + 1) * feats]
-            x_scaled[:, block * feats:(block + 1) * feats] = (wide * gain).astype(BF16)
+            x_scaled[:, span] = (wide * pre_ref[layer:layer + 1, span]).astype(BF16)
+            if layer == 0 and shift == min(1, n_tp - 1):
+                pass_on(order[2])
+                pass_across(order[1])
         inverse = lax.rsqrt(total / d_model + EPS)
 
         if layer == 0:
+            pass_on(order[3])
             pass_across(order[2])
         for which in order[:3]:
             finish_weight(base + which)
@@ -280,8 +289,7 @@
             for slot in order:
                 start_weight(base + 4 + slot)
         if layer == 0:
-            pass_on(3)
-            pass_across(3)
+            pass_across(order[3])
 
         for which in range(2):
             @pl.when(has_next)
@@ -353,6 +361,7 @@
         if layer + 1 < layers:
             for slot in order:
                 pass_on(base + 4 + slot)
+            expand_layer(layer + 1)
         branch = part[layer, tp].astype(F32)
         for shift in range(1, n_tp):
             for row in range(rows_dev):
@@ -416,14 +425,14 @@
     n_pair = width // 128
     d_model = feats * n_tp
     n_off = 2 * NA_ROWS - 2
-    doc_query = jnp.broadcast_to(documents[:, None], (tokens, 128))
     grid_docs = documents.reshape(rows_dev, 1, GRID_W)
     doc_key = jnp.broadcast_to(
         jnp.concatenate([grid_docs, grid_docs], axis=2), (rows_dev, 8, 2 * GRID_W)
     )
-    table = jnp.pad(offset_bias, ((0, 0), (0, 0), (0, 0), (0, GRID_W - 2 * NA_COLS + 1)))
-    table = jnp.concatenate([table[:, :, :-1], table[:, :, 1:]], axis=3)
-    table = table.reshape(layers * n_pair, 2, n_off, 128).transpose(0, 2, 1, 3)
+    table = jnp.pad(
+        offset_bias.reshape(layers * n_pair * 2, 2 * NA_ROWS - 1, 2 * NA_COLS - 1),
+        ((0, 0), (0, 1), (0, 128 - 2 * NA_COLS + 1)),
+    )
     n_y = n_sp // 2
     slots = 4 * layers
     ext = tokens + 2 * HALO
@@ -433,7 +442,7 @@
     return pl.pallas_call(
         functools.partial(kernel, n_sp, n_tp, n_grp, layers, tokens),
         out_shape=jax.ShapeDtypeStruct((tokens, feats), BF16),
-        in_specs=[vmem] * 3 + [hbm] * 4 + [vmem] * 3,
+        in_specs=[vmem] * 2 + [hbm] * 4 + [vmem] * 3,
         out_specs=vmem,
         scratch_shapes=[
             pltpu.VMEM((slots, d_model, width), BF16),
@@ -466,7 +475,7 @@
             collective_id=0, has_side_effects=True, vmem_limit_bytes=60 * 1024 * 1024
         ),
     )(
-        stream, doc_query, doc_key, q_weight, k_weight, v_weight, out_weight,
+        stream, doc_key, q_weight, k_weight, v_weight, out_weight,
         pre_gain, post_gain, table,
     )
 

time: 145 us -> 145 us (level)
  Pallas kernels: 138 us -> 140 us
    pallas_call x1, Pallas kernels: 138 us -> 140 us  [shards(): pl.pallas_call(functools.partial(kernel, n_sp, n_tp, n_grp, layers, token...]
where the time goes in v2:
time: 145 us; the launch traced here: 144 us
  Pallas kernels  140 us (97%)
  local copies, waits for them, and re-layouts  4.63 us (3%)
    pallas_call x1, Pallas kernels, shards(): pl.pallas_call(functools.partial(kernel, n_sp, n_tp, n_grp, layers, token...  140 us

profile of v2, /device:TPU:4, one launch (start us, length us, event | category | flops | bytes accessed | tf_op | source)
XLA Modules:
  0.0 144.5 jit_solution(8383906205411722512)
XLA Ops:
  0.0 0.8 reshape.6
  0.8 0.1 add_bitcast_fusion
  0.8 0.6 broadcast_in_dim.8.dock_ref
  1.4 0.9 copy.10
  2.4 0.7 pad.4.tab_ref
  3.0 139.7 %shard_map.91 = bf16[256,512]{1,0:T(8,128)(2,1)} custom-call(bf16[256,512]{1,0:T(8,128)(2,1)} %x_ref.1, s32[4,8,128]{2,1,0:T(8,128)} %broadcast_in_dim.8.dock_ref, bf16[2,512,512]{2,1,0:T(8,128)(2,1)} %wq_ref.1, bf16[2,512,512]{2,1,0:T(8,128)(2,1)} %wk_ref.1, bf16[2,512,512]{2,1,0:T(8,128)(2,1)} %wv_ref.1, bf16[2,512,512]{2,1,0:T(8,128)(2,1)} %wo_ref.1, ...), custom_call_target="tpu_custom_call" | custom-call | tf_op jit(solution)/shard_map/pallas_call | solution.py:442
  142.8 1.7 %copy.12 = bf16[256,512]{1,0:T(8,128)(2,1)} copy(bf16[256,512]{1,0:T(8,128)(2,1)} %shard_map.91) | data formatting | bytes 524288

commit v3 on v2

--- a/solution.py
+++ b/solution.py
@@ -169,7 +169,7 @@
     has_next, has_prev = sp < n_sp - 1, sp > 0
 
     order = (1, 2, 0, 3)
-    for slot in order:
+    for slot in order[:3]:
         start_weight(slot)
     x_local = pltpu.make_async_copy(x_ref, x_full.at[0, tp], xl_sem)
     x_local.start()
@@ -245,6 +245,7 @@
             dmask[row, pair, GRID_W:2 * GRID_W] = value
 
     pass_on(order[1])
+    start_weight(order[3])
     pass_across(order[0])
     x_local.wait()
 
@@ -359,9 +360,9 @@
         lax.fori_loop(0, rows_dev, attend, 0)
 
         if layer + 1 < layers:
+            expand_layer(layer + 1)
             for slot in order:
                 pass_on(base + 4 + slot)
-            expand_layer(layer + 1)
         branch = part[layer, tp].astype(F32)
         for shift in range(1, n_tp):
             for row in range(rows_dev):

time: 145 us -> 138 us (0.952)
  Pallas kernels: 140 us -> 131 us
    pallas_call x1, Pallas kernels: 140 us -> 131 us  [shards(): pl.pallas_call(functools.partial(kernel, n_sp, n_tp, n_grp, layers, token...]
where the time goes in v3:
time: 138 us; the launch traced here: 136 us
  Pallas kernels  131 us (95%)
  local copies, waits for them, and re-layouts  4.63 us (3%)
    pallas_call x1, Pallas kernels, shards(): pl.pallas_call(functools.partial(kernel, n_sp, n_tp, n_grp, layers, token...  131 us

profile of v3, /device:TPU:4, one launch (start us, length us, event | category | flops | bytes accessed | tf_op | source)
XLA Modules:
  0.0 136.2 jit_solution(8939849485047400771)
XLA Ops:
  0.0 0.8 reshape.6
  0.8 0.1 add_bitcast_fusion
  0.8 0.6 broadcast_in_dim.8.dock_ref
  1.4 0.9 copy.10
  2.4 0.7 pad.4.tab_ref
  3.0 131.4 %shard_map.91 = bf16[256,512]{1,0:T(8,128)(2,1)} custom-call(bf16[256,512]{1,0:T(8,128)(2,1)} %x_ref.1, s32[4,8,128]{2,1,0:T(8,128)} %broadcast_in_dim.8.dock_ref, bf16[2,512,512]{2,1,0:T(8,128)(2,1)} %wq_ref.1, bf16[2,512,512]{2,1,0:T(8,128)(2,1)} %wk_ref.1, bf16[2,512,512]{2,1,0:T(8,128)(2,1)} %wv_ref.1, bf16[2,512,512]{2,1,0:T(8,128)(2,1)} %wo_ref.1, ...), custom_call_target="tpu_custom_call" | custom-call | tf_op jit(solution)/shard_map/pallas_call | solution.py:443
  134.5 1.7 %copy.12 = bf16[256,512]{1,0:T(8,128)(2,1)} copy(bf16[256,512]{1,0:T(8,128)(2,1)} %shard_map.91) | data formatting | bytes 524288

commit v4 on v3

--- a/solution.py
+++ b/solution.py
@@ -289,8 +289,6 @@
         if layer + 1 < layers:
             for slot in order:
                 start_weight(base + 4 + slot)
-        if layer == 0:
-            pass_across(order[3])
 
         for which in range(2):
             @pl.when(has_next)
@@ -300,8 +298,6 @@
             @pl.when(has_prev)
             def _():
                 halo_copy(layer, 0, which).wait_recv()
-
-        finish_weight(base + 3)
 
         def r_copy(row, shift):
             here = pl.ds(pl.multiple_of(row * GRID_W, GRID_W), GRID_W)
@@ -345,6 +341,13 @@
                     jnp.where(low_half, mixed[:GRID_W], mixed[GRID_W:]).astype(BF16)
                 )
             attended = jnp.concatenate(attended, axis=1)
+
+            @pl.when(row == 0)
+            def _():
+                if layer == 0:
+                    pass_across(order[3])
+                finish_weight(base + 3)
+
             for shift in list(range(1, n_tp)) + [0]:
                 block = tp_at(shift)
                 w_rows = pl.ds(pl.multiple_of(block * feats, feats), feats)

time: 138 us -> 144 us (1.043); the launches traced: 136 us -> 144 us
  Pallas kernels: 131 us -> 139 us
    pallas_call x1, Pallas kernels: 131 us -> 139 us  [shards(): pl.pallas_call(functools.partial(kernel, n_sp, n_tp, n_grp, layers, token...]
where the time goes in v4:
time: 144 us
  Pallas kernels  139 us (97%)
  local copies, waits for them, and re-layouts  4.63 us (3%)
    pallas_call x1, Pallas kernels, shards(): pl.pallas_call(functools.partial(kernel, n_sp, n_tp, n_grp, layers, token...  139 us

profile of v4, /device:TPU:4, one launch (start us, length us, event | category | flops | bytes accessed | tf_op | source)
XLA Modules:
  0.0 144.0 jit_solution(14189015079288461809)
XLA Ops:
  0.0 0.8 reshape.6
  0.8 0.1 add_bitcast_fusion
  0.8 0.6 broadcast_in_dim.8.dock_ref
  1.4 0.9 copy.10
  2.4 0.7 pad.4.tab_ref
  3.0 139.3 %shard_map.91 = bf16[256,512]{1,0:T(8,128)(2,1)} custom-call(bf16[256,512]{1,0:T(8,128)(2,1)} %x_ref.1, s32[4,8,128]{2,1,0:T(8,128)} %broadcast_in_dim.8.dock_ref, bf16[2,512,512]{2,1,0:T(8,128)(2,1)} %wq_ref.1, bf16[2,512,512]{2,1,0:T(8,128)(2,1)} %wk_ref.1, bf16[2,512,512]{2,1,0:T(8,128)(2,1)} %wv_ref.1, bf16[2,512,512]{2,1,0:T(8,128)(2,1)} %wo_ref.1, ...), custom_call_target="tpu_custom_call" | custom-call | tf_op jit(solution)/shard_map/pallas_call | solution.py:446
  142.4 1.7 %copy.12 = bf16[256,512]{1,0:T(8,128)(2,1)} copy(bf16[256,512]{1,0:T(8,128)(2,1)} %shard_map.91) | data formatting | bytes 524288
